TPU v7x, 256 devices: a whole 4x4x8 slice. The times are simulated.
256 devices in a mesh: sp: 16 (over y, x), tp: 16 (over z, core).
Axes of the slice: x: 4, y: 4, z: 8, core: 2. Of those that a mesh axis runs over, the one named last changes fastest.
Arguments:
- layer_in: bfloat16 [5120, 2048], P('sp', 'tp'), may hold values from -6 to 6
- out_cot: bfloat16 [5120, 2048], P('sp', 'tp'), may hold values from -6 to 6
- route_ids: int32 [5120, 2], P('sp'), may hold values from 0 to 15, all different within a row; in each aligned block of 320 rows (0 to 319, 320 to 639, ...) at most 80 rows name the same one
- route_probs: float32 [5120, 2], P('sp'), may hold values from 0.2 to 1
- group_prob: float32 [5120], P('sp'), may hold values from 0.3 to 1
- gate_weight: bfloat16 [16, 2048, 2048], P('sp', 'tp'), may hold values from -0.125 to 0.125
- up_weight: bfloat16 [16, 2048, 2048], P('sp', 'tp'), may hold values from -0.125 to 0.125
- down_weight: bfloat16 [16, 2048, 2048], P('sp', 'tp'), may hold values from -0.125 to 0.125
- out_weight: bfloat16 [2048, 2048], P(None, 'tp'), may hold values from -0.125 to 0.125
- query: bfloat16 [5120, 1024], P('sp', 'tp'), may hold values from -6 to 6
- key_in: bfloat16 [5120, 1024], P('sp', 'tp'), may hold values from -0.75 to 0.75
- value: bfloat16 [5120, 2048], P('sp', 'tp'), may hold values from -6 to 6
- decay_logit: bfloat16 [5120, 1024], P('sp', 'tp'), may hold values from -2.5 to 8.5, as said below
Outputs:
- gate_grad: float32 [16, 2048, 2048], P('sp', 'tp')
- up_grad: float32 [16, 2048, 2048], P('sp', 'tp')
- down_grad: float32 [16, 2048, 2048], P('sp', 'tp')
- proj_grad: float32 [2048, 2048], P('sp', 'tp')
- query_grad: float32 [5120, 1024], P('sp', 'tp')
- key_grad: float32 [5120, 1024], P('sp', 'tp')
- value_grad: float32 [5120, 2048], P('sp', 'tp')
- logit_grad: float32 [5120, 1024], P('sp', 'tp')
Inputs may be any that keep to these rules, and one draw needn't show every extreme that they name: `route_ids`: each row names two different experts of 0 to 15; every expert is named by some row; within each aligned block of 320 rows (the rows of one device) no expert is named more than 80 times, and in some block one expert is named exactly 80 times. `decay_logit`: values lie between -2.5 and 8.5; even heads have pre-activations near 5, odd heads near 1.
All inputs are finite; a program needn't handle non-finite values.
Results may differ from a plain program's by a relative error of at most 0.019.
Values may be sent and summed in bfloat16 or wider, within the bound.
No kernel may reach another device: no remote copies, remote signals or barrier semaphores. Data moves between devices by JAX's collectives and lax.ppermute only.
A program may use at most 128 MiB of HBM per device.

v0:
```python
import jax
import jax.numpy as jnp
from jax import lax
from jax.sharding import PartitionSpec as P

DK = 64
DV = 128
BLOCK = 64
decay_temp = 16.0
highest = lax.Precision.HIGHEST


def side_by_side(arrays, axis, dim, along):
    both = jnp.concatenate(arrays, axis=along)
    filled, at, finished = (lax.all_gather(both, axis, axis=dim, tiled=True), 0, [])
    for a in arrays:
        finished.append(lax.slice_in_dim(filled, at, at + a.shape[along], axis=along))
        at += a.shape[along]
    return tuple(finished)


def side_by_side_2(arrays, axis, split_dim, concat_dim, along):
    widths = [a.shape[along] for a in arrays]
    both = jnp.concatenate(arrays, axis=along)
    filled = lax.all_to_all(both, axis, split_axis=split_dim, concat_axis=concat_dim, tiled=True)
    return tuple(jnp.split(filled, [sum(widths[:k]) for k in range(1, len(widths))], axis=along))


def sent_to_all(x, axis):
    copies = jnp.broadcast_to(x, (lax.axis_size(axis), *x.shape))
    return lax.all_to_all(copies, axis, split_axis=0, concat_axis=0, tiled=True)


def all_in_one(x, axis):
    leaves = jax.tree.leaves(x)
    turns = sorted(range(len(leaves)), key=lambda k: -leaves[k].size)
    width = (1, *leaves[turns[0]].shape)[-1]
    lines = [
        jnp.pad(leaves[k].reshape(-1), (0, -leaves[k].size % width)).reshape(-1, width)
        for k in turns
    ]
    both, at, found = (sent_to_all(jnp.concatenate(lines), axis), 0, {})
    for k, line in zip(turns, lines):
        section = both[:, at : at + len(line)].reshape(len(both), -1)
        found[k] = section[:, : leaves[k].size].reshape(-1, *leaves[k].shape)
        at += len(line)
    numbers = iter(range(len(leaves)))
    return jax.tree.map(lambda _: found[next(numbers)], x)


def folded_in_pairs(pieces, combine):
    while len(jax.tree.leaves(pieces)[0]) > 1:
        pieces = jax.vmap(combine)(
            *(jax.tree.map(lambda part: part[side::2], pieces) for side in (0, 1))
        )
    return jax.tree.map(lambda part: part[0], pieces)


def entering(x, axis, combine, identity, reverse):
    length, index = (lax.axis_size(axis), lax.axis_index(axis))
    passed = jnp.arange(length) > index if reverse else jnp.arange(length) < index

    def kept(part, zero, own):
        part = jnp.where(
            passed.reshape(-1, *(1 for _ in own.shape)),
            part.astype(own.dtype),
            jnp.asarray(zero, own.dtype),
        )
        return part[::-1] if reverse else part

    pieces = all_in_one(
        jax.tree.map(
            lambda part, kind: part.astype(kind),
            x,
            jax.tree.map(lambda a: jnp.bfloat16 if a.dtype == jnp.float32 else a.dtype, x),
        ),
        axis,
    )
    return folded_in_pairs(jax.tree.map(kept, pieces, identity, x), combine)


def in_blocks(x, dim, length):
    lengths = x.shape
    blocks = x.reshape(*lengths[:dim], length, lengths[dim] // length, *lengths[dim + 1 :])
    return jnp.moveaxis(blocks, dim, 0)


def summed_on_arrival(x, axis, dim):
    length = lax.axis_size(axis)
    blocks = lax.all_to_all(in_blocks(x, dim, length), axis, 0, 0, tiled=True)
    return jnp.sum(blocks.astype(jnp.float32), axis=0)


def combine_spans(earlier, later):
    return (earlier[0] * later[0], later[1] + later[0][..., None] * earlier[1])


def contract_rows(left_mat, right_mat):
    return lax.dot_general(
        left_mat, right_mat, (((0,), (0,)), ((), ())), preferred_element_type=jnp.float32
    )


def contract_cols(left_mat, right_mat):
    return lax.dot_general(
        left_mat, right_mat, (((1,), (1,)), ((), ())), preferred_element_type=jnp.float32
    )


def to_blocks(tensor, head_count):
    rows_here = tensor.shape[0]
    return (
        tensor.astype(jnp.float32)
        .reshape(rows_here // BLOCK, BLOCK, head_count, -1)
        .transpose(2, 0, 1, 3)
    )


def from_blocks(tensor):
    head_count, blocks, _, channels = tensor.shape
    return tensor.transpose(1, 2, 0, 3).reshape(blocks * BLOCK, head_count * channels)


def expert_pass(rows_x, rows_cot, gate_mat, up_mat, down_mat):
    full_x, full_cot = side_by_side((rows_x, rows_cot), "tp", 1, 0)
    gate_pre = contract_cols(full_x, gate_mat)
    up_pre = contract_cols(full_x, up_mat)
    sigmoid_gate = jax.nn.sigmoid(gate_pre)
    active = gate_pre * sigmoid_gate
    hidden = (active * up_pre).astype(jnp.bfloat16)
    hidden_cot = contract_cols(full_cot, down_mat)
    up_cot = (hidden_cot * active).astype(jnp.bfloat16)
    gate_cot = (
        hidden_cot * up_pre * sigmoid_gate * (1.0 + gate_pre * (1.0 - sigmoid_gate))
    ).astype(jnp.bfloat16)
    down_g = contract_rows(hidden, full_cot)
    gate_g = contract_rows(gate_cot, full_x)
    up_g = contract_rows(up_cot, full_x)
    dims = (((0,), (1,)), ((), ()))
    first_part = lax.dot_general(gate_mat, gate_cot, dims, preferred_element_type=jnp.float32)
    back_terms = lax.psum_scatter(
        (
            first_part + lax.dot_general(up_mat, up_cot, dims, preferred_element_type=jnp.float32)
        ).astype(jnp.bfloat16),
        "tp",
        scatter_dimension=0,
        tiled=True,
    ).astype(jnp.float32)
    return (gate_g, up_g, down_g, back_terms)


def local(
    layer_in,
    out_cot,
    route_ids,
    route_probs,
    group_prob,
    gate_weight,
    up_weight,
    down_weight,
    out_weight,
    query,
    key_in,
    value,
    decay_logit,
):
    tok_rows = layer_in.shape[0]
    local_cols = layer_in.shape[1]
    experts_all = lax.axis_size("sp")
    capacity = 4 * tok_rows // experts_all
    route_weight = group_prob[:, None] * route_probs / jnp.sum(route_probs, axis=1, keepdims=True)
    chosen = (route_ids[:, :, None] == jnp.arange(experts_all, dtype=jnp.int32)).astype(jnp.int32)
    running = jnp.cumsum(chosen.reshape(2 * tok_rows, experts_all), axis=0).reshape(
        tok_rows, 2, experts_all
    )
    position = jnp.sum((running - 1) * chosen, axis=2)
    slot_ids = route_ids * capacity + position
    matches = (
        slot_ids[None, :, :] == jnp.arange(experts_all * capacity, dtype=jnp.int32)[:, None, None]
    )
    select_x = jnp.any(matches, axis=2).astype(jnp.float32)
    select_cot = jnp.sum(jnp.where(matches, route_weight[None], 0.0), axis=2)
    send_x = jnp.dot(
        select_x.astype(jnp.bfloat16), layer_in, preferred_element_type=jnp.float32
    ).astype(jnp.bfloat16)
    send_cot = jnp.dot(select_cot, out_cot.astype(jnp.float32), precision=highest).astype(
        jnp.bfloat16
    )
    send_x = send_x.reshape(experts_all, capacity, local_cols)
    send_cot = send_cot.reshape(experts_all, capacity, local_cols)
    recv_x, recv_cot = side_by_side_2((send_x, send_cot), "sp", 0, 0, 1)
    head_dev = query.shape[1] // DK
    scaled_query = to_blocks(query, head_dev) * DK ** (-0.5)
    key_blk = to_blocks(key_in, head_dev)
    value_blk = to_blocks(value, head_dev)
    logit_blk = to_blocks(decay_logit, head_dev)
    cumulative = jnp.cumsum(jax.nn.log_sigmoid(logit_blk) / decay_temp, axis=2)
    span_log = cumulative[:, :, -1:, :]
    growth = jnp.exp(cumulative)
    shrink = jnp.exp(-cumulative)
    to_end = jnp.exp(span_log - cumulative)
    query_decayed = scaled_query * growth
    key_back = key_blk * shrink
    key_to_end = key_blk * to_end
    causal = jnp.tril(jnp.ones((BLOCK, BLOCK), dtype=bool))
    scores = jnp.where(
        causal, jnp.einsum("hncd,hnsd->hncs", query_decayed, key_back, precision=highest), 0.0
    )
    within = jnp.einsum("hncs,hnsv->hncv", scores, value_blk, precision=highest)
    block_decay = jnp.moveaxis(jnp.exp(span_log[:, :, 0, :]), 1, 0)
    block_update = jnp.moveaxis(
        jnp.einsum("hncd,hncv->hndv", key_to_end, value_blk, precision=highest), 1, 0
    )
    identity_pair = (
        jnp.ones((head_dev, DK), jnp.float32),
        jnp.zeros((head_dev, DK, DV), jnp.float32),
    )

    def advance(carry_pair, inputs):
        return (combine_spans(carry_pair, inputs), carry_pair)

    span_total, before_pairs = lax.scan(advance, identity_pair, (block_decay, block_update))
    entry_pair = entering(span_total, "sp", combine_spans, identity_pair, False)
    entry_state = entry_pair[1]
    decay_before = jnp.moveaxis(before_pairs[0], 0, 1)
    block_state = decay_before[..., None] * entry_state[:, None] + jnp.moveaxis(
        before_pairs[1], 0, 1
    )
    span_end = span_total[0][..., None] * entry_state + span_total[1]
    outputs = within + jnp.einsum("hncd,hndv->hncv", query_decayed, block_state, precision=highest)
    mixer_out = from_blocks(outputs).astype(jnp.bfloat16)
    gate_mat, up_mat, down_mat = (gate_weight[0], up_weight[0], down_weight[0])
    gate_g, up_g, down_g, back_flat = expert_pass(
        recv_x.reshape(-1, local_cols), recv_cot.reshape(-1, local_cols), gate_mat, up_mat, down_mat
    )
    back_terms = back_flat.reshape(local_cols, experts_all, capacity)
    returned = lax.all_to_all(
        back_terms.astype(jnp.bfloat16), "sp", split_axis=1, concat_axis=1, tiled=True
    ).astype(back_terms.dtype)
    returned = returned.reshape(local_cols, experts_all * capacity)
    routed_sum = lax.dot_general(
        select_x,
        returned,
        (((0,), (1,)), ((), ())),
        precision=highest,
        preferred_element_type=jnp.float32,
    )
    mixed_cot = (out_cot.astype(jnp.float32) + routed_sum).astype(jnp.bfloat16)
    full_cot = lax.all_gather(mixed_cot, "tp", axis=1, tiled=True)
    mixer_cot = jnp.dot(full_cot, out_weight, preferred_element_type=jnp.float32)
    proj_grad = summed_on_arrival(contract_rows(full_cot, mixer_out).astype(jnp.bfloat16), "sp", 0)
    cot_blk = to_blocks(mixer_cot, head_dev)
    block_future = jnp.moveaxis(
        jnp.einsum("hncd,hncv->hndv", query_decayed, cot_blk, precision=highest), 1, 0
    )

    def retreat(carry_pair, inputs):
        return (combine_spans(carry_pair, inputs), carry_pair)

    span_back, after_pairs = lax.scan(
        retreat, identity_pair, (block_decay, block_future), reverse=True
    )
    beyond_pair = entering(span_back, "sp", combine_spans, identity_pair, True)
    future_state = beyond_pair[1]
    decay_after = jnp.moveaxis(after_pairs[0], 0, 1)
    block_future_state = decay_after[..., None] * future_state[:, None] + jnp.moveaxis(
        after_pairs[1], 0, 1
    )
    cot_values = jnp.where(
        causal, jnp.einsum("hncv,hnsv->hncs", cot_blk, value_blk, precision=highest), 0.0
    )
    query_scaled_grad = growth * (
        jnp.einsum("hncv,hndv->hncd", cot_blk, block_state, precision=highest)
        + jnp.einsum("hncs,hnsd->hncd", cot_values, key_back, precision=highest)
    )
    key_part = shrink * jnp.einsum("hncs,hncd->hnsd", cot_values, query_decayed, precision=highest)
    key_grad = key_part + to_end * jnp.einsum(
        "hnsv,hndv->hnsd", value_blk, block_future_state, precision=highest
    )
    value_grad = jnp.einsum("hncs,hncv->hnsv", scores, cot_blk, precision=highest) + jnp.einsum(
        "hnsd,hndv->hnsv", key_to_end, block_future_state, precision=highest
    )
    decay_terms = (scaled_query * query_scaled_grad - key_blk * key_grad).reshape(
        head_dev, tok_rows, DK
    )
    tail_sum = jnp.flip(jnp.cumsum(jnp.flip(decay_terms, 1), axis=1), 1)
    beyond_term = jnp.sum(future_state * span_end, axis=2)
    log_grad = tail_sum + beyond_term[:, None, :]
    logit_flat = logit_blk.reshape(head_dev, tok_rows, DK)
    logit_grad = (
        (log_grad * jax.nn.sigmoid(-logit_flat) / decay_temp)
        .transpose(1, 0, 2)
        .reshape(tok_rows, head_dev * DK)
    )
    query_grad = from_blocks(query_scaled_grad * DK ** (-0.5))
    return (
        gate_g[None],
        up_g[None],
        down_g[None],
        proj_grad,
        query_grad,
        from_blocks(key_grad),
        from_blocks(value_grad),
        logit_grad,
    )


def solution(mesh):
    in_specs = (
        P("sp", "tp"),
        P("sp", "tp"),
        P("sp", None),
        P("sp", None),
        P("sp"),
        P("sp", "tp", None),
        P("sp", "tp", None),
        P("sp", "tp", None),
        P(None, "tp"),
        P("sp", "tp"),
        P("sp", "tp"),
        P("sp", "tp"),
        P("sp", "tp"),
    )
    out_specs = (
        P("sp", "tp", None),
        P("sp", "tp", None),
        P("sp", "tp", None),
        P("sp", "tp"),
        P("sp", "tp"),
        P("sp", "tp"),
        P("sp", "tp"),
        P("sp", "tp"),
    )
    return jax.shard_map(local, mesh=mesh, in_specs=in_specs, out_specs=out_specs, check_vma=False)
```

profile of v0, /device:TPU:32, one launch (start us, length us, event | category | flops | bytes accessed | tf_op | source)
XLA Modules:
  0.0 299.6 jit_solution(3981683871783346753)
XLA Ops:
  8.4 1.4 reduce-window.14
  13.5 2.7 convolution_convert_fusion.1
  16.1 1.4 convolution_convert_fusion.2
  17.5 19.8 %all_to_all.25 = bf16[16,160,128]{2,1,0:T(8,128)(2,1)S(1)} all-to-all(bf16[16,160,128]{2,1,0:T(8,128)(2,1)S(1)} %pad_maximum_fusion), channel_id=1, replica_groups=mesh['sp'=16,'tp'=16] {'sp'}, dimensions={0} | all-to-all | bytes 1310720 | tf_op jit(solution)/shard_map/all_to_all | solution.py:25
  38.5 71.1 %all-gather.3.cloned.1.call-done = bf16[2560,2048]{1,0:T(8,128)(2,1)} async-done(((bf16[2560,128]{1,0:T(8,128)(2,1)}), bf16[2560,2048]{1,0:T(8,128)(2,1)}) %all-gather.3.cloned.1.call-update) | async-done | bytes 10485776 | tf_op jit(solution)/shard_map/all_gather | solution.py:15
  109.6 4.2 %fusion.13 = f32[1280,128]{1,0:T(8,128)S(1)} fusion(bf16[2560,2048]{1,0:T(8,128)(2,1)} %all-gather.3.cloned.1.call-done, bf16[1,128,2048]{2,1,0:T(8,128)(2,1)S(1)} %copy-done), kind=kOutput, calls=%fused_computation.24 | convolution fusion | flops 671088640 | bytes 6422528 | tf_op jit(solution)/shard_map/dot_general | solution.py:105
  113.8 1.3 copy-done.1
  115.2 1.6 fusion.15
  116.8 1.7 multiply_convert_fusion.1
  118.5 1.5 fusion.33
  120.0 3.8 %fusion.4 = bf16[2048,1280]{0,1:T(8,128)(2,1)} fusion(f32[1280,2048]{1,0:T(8,128)S(1)} %fusion.33, bf16[1280,128]{1,0:T(8,128)(2,1)S(1)} %get-tuple-element.412, bf16[1,128,2048]{2,1,0:T(8,128)(2,1)S(1)} %copy-done.6), kind=kOutput, calls=%fused_computation.15 | convolution fusion | flops 676331520 | bytes 16580608 | tf_op jit(solution)/shard_map/dot_general | solution.py:143
  123.8 7.9 %copy.182 = bf16[2048,1280]{1,0:T(8,128)(2,1)} copy(bf16[2048,1280]{0,1:T(8,128)(2,1)} %fusion.4) | data formatting | bytes 10485760
  135.1 6.0 %all-to-all-start.2 = ((bf16[16,65,128]{2,1,0:T(8,128)(2,1)}), bf16[16,65,128]{2,1,0:T(8,128)(2,1)S(1)}, u32[]{:S(2)}, u32[]{:S(2)}) async-start(bf16[16,65,128]{2,1,0:T(8,128)(2,1)} %broadcast_in_dim.136), calls=%async_computation.2 | async-start | bytes 589824 | tf_op jit(solution)/shard_map/all_to_all | solution.py:31
  142.4 8.1 %all-to-all-done.2 = bf16[16,65,128]{2,1,0:T(8,128)(2,1)S(1)} async-done(((bf16[16,65,128]{2,1,0:T(8,128)(2,1)}), bf16[16,65,128]{2,1,0:T(8,128)(2,1)S(1)}, u32[]{:S(2)}, u32[]{:S(2)}) %all-to-all-start.2) | async-done | bytes 266272 | tf_op jit(solution)/shard_map/all_to_all | solution.py:31
  150.6 41.9 %reduce-scatter.4.cloned.1.call-done = bf16[128,1280]{1,0:T(8,128)(2,1)} async-done(((bf16[2048,1280]{1,0:T(8,128)(2,1)}), bf16[128,1280]{1,0:T(8,128)(2,1)}) %reduce-scatter.4.cloned.1.call-update) | async-done | bytes 327696
  192.6 1.9 copy.183
  194.4 6.7 %all-to-all-start.1 = ((bf16[128,16,80]{0,2,1:T(8,128)(2,1)}), bf16[128,16,80]{0,2,1:T(8,128)(2,1)}, u32[]{:S(2)}, u32[]{:S(2)}) async-start(bf16[128,16,80]{0,2,1:T(8,128)(2,1)} %bitcast.12), calls=%async_computation.1 | async-start | bytes 655360 | tf_op jit(solution)/shard_map/all_to_all | solution.py:237
  201.7 8.5 %all-to-all-done.1 = bf16[128,16,80]{0,2,1:T(8,128)(2,1)} async-done(((bf16[128,16,80]{0,2,1:T(8,128)(2,1)}), bf16[128,16,80]{0,2,1:T(8,128)(2,1)}, u32[]{:S(2)}, u32[]{:S(2)}) %all-to-all-start.1) | async-done | bytes 327712 | tf_op jit(solution)/shard_map/all_to_all | solution.py:237
  210.2 2.1 fusion.31
  213.7 4.4 %fusion.18 = f32[1,128,2048]{2,1,0:T(8,128)} fusion(bf16[1280,128]{1,0:T(8,128)(2,1)S(1)} %get-tuple-element.413, bf16[2560,2048]{1,0:T(8,128)(2,1)} %all-gather.3.cloned.1.call-done), kind=kOutput, calls=%fused_computation.31 | convolution fusion | flops 671088640 | bytes 6619136 | tf_op jit(solution)/shard_map/dot_general | solution.py:99
  218.1 4.3 %fusion.21 = f32[1,128,2048]{2,1,0:T(8,128)} fusion(bf16[1280,128]{1,0:T(8,128)(2,1)S(1)} %get-tuple-element.412, bf16[2560,2048]{1,0:T(8,128)(2,1)} %all-gather.3.cloned.1.call-done), kind=kOutput, calls=%fused_computation.32 | convolution fusion | flops 671088640 | bytes 6619136 | tf_op jit(solution)/shard_map/dot_general | solution.py:99
  222.5 4.4 %fusion.24 = f32[1,128,2048]{2,1,0:T(8,128)} fusion(bf16[2560,2048]{1,0:T(8,128)(2,1)} %all-gather.3.cloned.1.call-done, f32[1280,128]{1,0:T(8,128)S(1)} %copy-done.20, f32[1280,128]{1,0:T(8,128)S(1)} %copy-done.18), kind=kOutput, calls=%fused_computation.33 | convolution fusion | flops 672071680 | bytes 7602176 | tf_op jit(solution)/shard_map/dot_general | solution.py:99
  226.9 21.5 %all-gather.5.cloned.1.call-done = bf16[320,2048]{1,0:T(8,128)(2,1)} async-done(((bf16[320,128]{1,0:T(8,128)(2,1)}), bf16[320,2048]{1,0:T(8,128)(2,1)}) %all-gather.5.cloned.1.call-update) | async-done | bytes 1310736 | tf_op jit(solution)/shard_map/all_gather | solution.py:249
  248.4 2.0 fusion.83
  253.5 7.3 %while.42 = (s32[]{:T(128)}, f32[1,64]{1,0:T(1,128)S(1)}, f32[1,64,128]{2,1,0:T(8,128)S(1)}, f32[5,1,64]{2,0,1:T(8,128)S(1)}, f32[5,1,64,128]{3,2,1,0:T(8,128)S(...) while((s32[]{:T(128)}, f32[1,64]{1,0:T(1,128)S(1)}, ...), condition=%wide.region_12.13_spmd.clone, body=%wide.region_11.12_spmd.clone.sunk | while | flops 32900 | bytes 166297 | solution.py:260
  261.5 6.8 %all-to-all-start.4 = ((bf16[16,65,128]{2,1,0:T(8,128)(2,1)}), bf16[16,65,128]{2,1,0:T(8,128)(2,1)S(1)}, u32[]{:S(2)}, u32[]{:S(2)}) async-start(bf16[16,65,128]{2,1,0:T(8,128)(2,1)} %broadcast_in_dim.141), calls=%async_computation.4 | async-start | bytes 589824 | tf_op jit(solution)/shard_map/all_to_all | solution.py:31
  268.3 2.3 convolution_convert_fusion
  271.8 1.9 fusion.29
  273.7 4.1 %all-to-all-done.4 = bf16[16,65,128]{2,1,0:T(8,128)(2,1)S(1)} async-done(((bf16[16,65,128]{2,1,0:T(8,128)(2,1)}), bf16[16,65,128]{2,1,0:T(8,128)(2,1)S(1)}, u32[]{:S(2)}, u32[]{:S(2)}) %all-to-all-start.4) | async-done | bytes 266272 | tf_op jit(solution)/shard_map/all_to_all | solution.py:31
  277.7 3.6 %all-to-all-start.3 = ((bf16[16,128,128]{2,1,0:T(8,128)(2,1)}), bf16[16,128,128]{2,1,0:T(8,128)(2,1)S(1)}, u32[]{:S(2)}, u32[]{:S(2)}) async-start(bf16[16,128,128]{2,1,0:T(8,128)(2,1)} %bitcast.35), calls=%async_computation.3 | async-start | bytes 1048576 | tf_op jit(solution)/shard_map/all_to_all | solution.py:90
  283.4 1.3 multiply_subtract_fusion
  290.9 1.4 all-to-all-done.3
  (214 shorter events, 34.2 us)
Async XLA Ops:
  7.2 102.5 %copy-start = (bf16[1,128,2048]{2,1,0:T(8,128)(2,1)S(1)}, bf16[1,128,2048]{2,1,0:T(8,128)(2,1)}, u32[]{:S(2)}) copy-start(bf16[1,128,2048]{2,1,0:T(8,128)(2,1)} %param.22) | copy-start | bytes 1572868
  7.2 102.4 %all-gather.3.cloned.1.call-start = ((), (), s32[]{:S(2)}) async-start(), calls=%async_computation.6 | async-start | bytes 11141120 | tf_op jit(solution)/shard_map/all_gather | solution.py:15
  11.6 26.6 %copy-start.7 = (pred[1280,320]{0,1:T(8,128)(4,1)}, pred[1280,320]{0,1:T(8,128)(4,1)S(1)}, u32[]{:S(2)}) copy-start(pred[1280,320]{0,1:T(8,128)(4,1)S(1)} %fusion.17) | copy-start | bytes 1228804
  38.3 75.5 %copy-start.6 = (bf16[1,128,2048]{2,1,0:T(8,128)(2,1)S(1)}, bf16[1,128,2048]{2,1,0:T(8,128)(2,1)}, u32[]{:S(2)}) copy-start(bf16[1,128,2048]{2,1,0:T(8,128)(2,1)} %param.23) | copy-start | bytes 1572868
  38.3 154.3 %reduce-scatter.4.cloned.1.call-start = ((), (), s32[]{:S(2)}) async-start(), calls=%async_computation.8 | async-start | bytes 5570560
  109.6 5.5 %copy-start.1 = (bf16[2560,2048]{1,0:T(8,128)(2,1)S(1)}, bf16[2560,2048]{1,0:T(8,128)(2,1)}, u32[]{:S(2)}) copy-start(bf16[2560,2048]{1,0:T(8,128)(2,1)} %all-gather.3.cloned.1.call-done) | copy-start | bytes 31457284
  115.2 1.6 copy-start.17
  115.2 1.6 copy-start.16
  116.7 1.7 copy-start.19
  131.7 0.8 copy-start.8
  131.7 0.9 copy-start.10
  131.7 1.3 copy-start.3
  131.7 9.4 %copy-start.9 = (bf16[320,64]{0,1:T(8,128)(2,1)S(1)}, bf16[320,64]{0,1:T(8,128)(2,1)}, u32[]{:S(2)}) copy-start(bf16[320,64]{0,1:T(8,128)(2,1)} %param.26) | copy-start | bytes 122884
  134.3 6.9 %copy-start.11 = (f32[5,1,64]{2,1,0:T(1,128)}, f32[5,1,64]{2,1,0:T(1,128)S(1)}, u32[]{:S(2)}) copy-start(f32[5,1,64]{2,1,0:T(1,128)S(1)} %get-tuple-element.589) | copy-start | bytes 3844
  134.3 78.2 %copy-start.12 = (f32[1,64]{1,0:T(1,128)}, f32[1,64]{1,0:T(1,128)S(1)}, u32[]{:S(2)}) copy-start(f32[1,64]{1,0:T(1,128)S(1)} %get-tuple-element.194) | copy-start | bytes 772
  135.1 15.4 %all-to-all-start.2 = ((bf16[16,65,128]{2,1,0:T(8,128)(2,1)}), bf16[16,65,128]{2,1,0:T(8,128)(2,1)S(1)}, u32[]{:S(2)}, u32[]{:S(2)}) async-start(bf16[16,65,128]{2,1,0:T(8,128)(2,1)} %broadcast_in_dim.136), calls=%async_computation.2 | async-start | bytes 589824 | tf_op jit(solution)/shard_map/all_to_all | solution.py:31
  194.4 15.8 %all-to-all-start.1 = ((bf16[128,16,80]{0,2,1:T(8,128)(2,1)}), bf16[128,16,80]{0,2,1:T(8,128)(2,1)}, u32[]{:S(2)}, u32[]{:S(2)}) async-start(bf16[128,16,80]{0,2,1:T(8,128)(2,1)} %bitcast.12), calls=%async_computation.1 | async-start | bytes 655360 | tf_op jit(solution)/shard_map/all_to_all | solution.py:237
  201.1 47.3 %all-gather.5.cloned.1.call-start = ((), (), s32[]{:S(2)}) async-start(), calls=%async_computation.7 | async-start | bytes 1392640 | tf_op jit(solution)/shard_map/all_gather | solution.py:249
  212.4 10.1 %copy-start.15 = (f32[64]{0:T(128)}, f32[64]{0:T(128)S(1)}, u32[]{:S(2)}) copy-start(f32[64]{0:T(128)S(1)} %slice_bitcast_fusion.1) | copy-start | bytes 772
  213.7 8.8 %copy-start.18 = (f32[1280,128]{1,0:T(8,128)S(1)}, f32[1280,128]{1,0:T(8,128)}, u32[]{:S(2)}) copy-start(f32[1280,128]{1,0:T(8,128)} %copy-done.17) | copy-start | bytes 1966084
  213.7 8.8 %copy-start.20 = (f32[1280,128]{1,0:T(8,128)S(1)}, f32[1280,128]{1,0:T(8,128)}, u32[]{:S(2)}) copy-start(f32[1280,128]{1,0:T(8,128)} %copy-done.19) | copy-start | bytes 1966084
  222.5 31.0 %copy-start.14 = (f32[1,64]{1,0:T(1,128)S(1)}, f32[1,64]{1,0:T(1,128)}, u32[]{:S(2)}) copy-start(f32[1,64]{1,0:T(1,128)} %custom-call.2) | copy-start | bytes 772
  248.4 19.9 %copy-start.2 = (bf16[320,2048]{1,0:T(8,128)(2,1)S(1)}, bf16[320,2048]{1,0:T(8,128)(2,1)}, u32[]{:S(2)}) copy-start(bf16[320,2048]{1,0:T(8,128)(2,1)} %all-gather.5.cloned.1.call-done) | copy-start | bytes 3932164
  261.5 16.2 %all-to-all-start.4 = ((bf16[16,65,128]{2,1,0:T(8,128)(2,1)}), bf16[16,65,128]{2,1,0:T(8,128)(2,1)S(1)}, u32[]{:S(2)}, u32[]{:S(2)}) async-start(bf16[16,65,128]{2,1,0:T(8,128)(2,1)} %broadcast_in_dim.141), calls=%async_computation.4 | async-start | bytes 589824 | tf_op jit(solution)/shard_map/all_to_all | solution.py:31
  268.3 18.3 %copy-start.13 = (f32[1,64]{1,0:T(1,128)S(1)}, f32[1,64]{1,0:T(1,128)}, u32[]{:S(2)}) copy-start(f32[1,64]{1,0:T(1,128)} %copy-done.12) | copy-start | bytes 772
  271.8 11.7 %copy-start.4 = (f32[5,64,64]{2,1,0:T(8,128)S(1)}, f32[5,64,64]{2,1,0:T(8,128)}, u32[]{:S(2)}) copy-start(f32[5,64,64]{2,1,0:T(8,128)} %convolution_multiply_fusion) | copy-start | bytes 245764
  277.7 14.6 %all-to-all-start.3 = ((bf16[16,128,128]{2,1,0:T(8,128)(2,1)}), bf16[16,128,128]{2,1,0:T(8,128)(2,1)S(1)}, u32[]{:S(2)}, u32[]{:S(2)}) async-start(bf16[16,128,128]{2,1,0:T(8,128)(2,1)} %bitcast.35), calls=%async_computation.3 | async-start | bytes 1048576 | tf_op jit(solution)/shard_map/all_to_all | solution.py:90
  282.9 7.0 %copy-start.5 = (f32[5,64,128]{2,1,0:T(8,128)S(1)}, f32[5,64,128]{2,1,0:T(8,128)}, u32[]{:S(2)}) copy-start(f32[5,64,128]{2,1,0:T(8,128)} %fusion.84) | copy-start | bytes 491524
Sparse Core Ops, SparseCore 0:
  38.4 71.1 all-gather.2
  131.9 60.6 reduce-scatter.3
  212.5 35.8 all-gather.4
where the time goes:
time: 301 us; the launch traced here: 300 us
  waiting for transfers between devices  157 us (52%)
  matrix products  46.6 us (15%)
  starting transfers between devices  23.5 us (8%)
  local copies, waits for them, and re-layouts  22.1 us (7%)
  blocking collectives  19.8 us (7%)
  other arithmetic  16.2 us (5%)
  between operations  14.5 us (5%)
    all_gather x1, waiting for transfers between devices, side_by_side(): lax.all_gather(both, axis, axis=dim, tiled=True)  71.1 us
    unnamed x4, waiting for transfers between devices  42 us
    all_gather x1, waiting for transfers between devices, local(): full_cot = lax.all_gather(mixed_cot, 'tp', axis=1, tiled=True)  21.5 us
    all_to_all x1, blocking collectives, side_by_side_2(): lax.all_to_all(both, axis, split_axis=split_dim, concat_axis=concat_dim,...  19.8 us
    dot_general x4, matrix products, contract_rows(): lax.dot_general(left_mat, right_mat, (((0,), (0,)), ((), ())), preferred_...  15.5 us
    unnamed x52, local copies, waits for them, and re-layouts  14.8 us
    all_to_all x2, starting transfers between devices, sent_to_all(): return lax.all_to_all(copies, axis, split_axis=0, concat_axis=0, tiled=True)  12.8 us
    all_to_all x2, waiting for transfers between devices, sent_to_all(): return lax.all_to_all(copies, axis, split_axis=0, concat_axis=0, tiled=True)  12.1 us
  transfers between devices with their start and end apart: 7, of which 7 were waited for; matrix products, arithmetic and copies ran while one was open for 11% of the time, Pallas kernels for 0%

commit v1 on v0

--- a/solution.py
+++ b/solution.py
@@ -8,6 +8,13 @@
 BLOCK = 64
 decay_temp = 16.0
 highest = lax.Precision.HIGHEST
+
+
+def lead_the_pipes(t0):
+    u_next = lax.axis_size("tp")
+    value_now = jnp.stack(u_next * [t0])
+    carry_out = lax.all_to_all(value_now, "tp", 0, 0)
+    return jnp.concatenate(carry_out, axis=1)
 
 
 def side_by_side(arrays, axis, dim, along):
@@ -246,7 +253,7 @@
         preferred_element_type=jnp.float32,
     )
     mixed_cot = (out_cot.astype(jnp.float32) + routed_sum).astype(jnp.bfloat16)
-    full_cot = lax.all_gather(mixed_cot, "tp", axis=1, tiled=True)
+    full_cot = lead_the_pipes(mixed_cot)
     mixer_cot = jnp.dot(full_cot, out_weight, preferred_element_type=jnp.float32)
     proj_grad = summed_on_arrival(contract_rows(full_cot, mixer_out).astype(jnp.bfloat16), "sp", 0)
     cot_blk = to_blocks(mixer_cot, head_dev)

time: 301 us -> 318 us (1.056)
  local copies, waits for them, and re-layouts: 22.1 us -> 28.4 us
  other arithmetic: 16.2 us -> 21.9 us
  starting transfers between devices: 23.5 us -> 28.1 us
    all_gather x1 -> x0, waiting for transfers between devices: 21.5 us -> none  [local(): full_cot = lax.all_gather(mixed_cot, 'tp', axis=1, tiled=True)]
    all_to_all x0 -> x1, waiting for transfers between devices: none -> 14.1 us  [lead_the_pipes(): carry_out = lax.all_to_all(value_now, 'tp', 0, 0)]
    unnamed x4 -> x3, waiting for transfers between devices: 42 us -> 50.4 us
    all_to_all x0 -> x1, starting transfers between devices: none -> 8.02 us  [lead_the_pipes(): carry_out = lax.all_to_all(value_now, 'tp', 0, 0)]
    all_to_all x2, waiting for transfers between devices: 12.1 us -> 7.29 us  [sent_to_all(): return lax.all_to_all(copies, axis, split_axis=0, concat_axis=0, tiled=True)]
    another operation x12 -> x14, local copies, waits for them, and re-layouts: 0.59 us -> 4.27 us
    unnamed x52 -> x70, local copies, waits for them, and re-layouts: 14.8 us -> 14.8 us
  transfers between devices with their start and end apart: 7 -> 7, of which waited for: 7 -> 6; matrix products, arithmetic and copies ran while one was open for 11% -> 10% of each run, Pallas kernels for 0% -> 0%
where the time goes in v1:
time: 318 us; the launch traced here: 314 us
  waiting for transfers between devices  155 us (49%)
  matrix products  45.6 us (14%)
  local copies, waits for them, and re-layouts  28.4 us (9%)
  starting transfers between devices  28.1 us (9%)
  other arithmetic  21.9 us (7%)
  blocking collectives  19.8 us (6%)
  between operations  14.8 us (5%)
    all_gather x1, waiting for transfers between devices, side_by_side(): lax.all_gather(both, axis, axis=dim, tiled=True)  71.1 us
    unnamed x3, waiting for transfers between devices  50.4 us
    all_to_all x1, blocking collectives, side_by_side_2(): lax.all_to_all(both, axis, split_axis=split_dim, concat_axis=concat_dim,...  19.8 us
    unnamed x70, local copies, waits for them, and re-layouts  14.8 us
    dot_general x4, matrix products, contract_rows(): lax.dot_general(left_mat, right_mat, (((0,), (0,)), ((), ())), preferred_...  14.7 us
    all_to_all x1, waiting for transfers between devices, lead_the_pipes(): carry_out = lax.all_to_all(value_now, 'tp', 0, 0)  14.1 us
    all_to_all x2, starting transfers between devices, sent_to_all(): return lax.all_to_all(copies, axis, split_axis=0, concat_axis=0, tiled=True)  9.62 us
    all_to_all x1, waiting for transfers between devices, local(): lax.all_to_all(back_terms.astype(jnp.bfloat16), 'sp', split_axis=1, conca...  8.12 us
  transfers between devices with their start and end apart: 7, of which 6 were waited for; matrix products, arithmetic and copies ran while one was open for 10% of the time, Pallas kernels for 0%

profile of v1, /device:TPU:32, one launch (start us, length us, event | category | flops | bytes accessed | tf_op | source)
XLA Modules:
  0.0 313.7 jit_solution(16199070898529048399)
XLA Ops:
  8.4 1.4 reduce-window.14
  14.8 2.7 convolution_convert_fusion.1
  17.5 19.8 %all_to_all.30 = bf16[16,160,128]{2,1,0:T(8,128)(2,1)S(1)} all-to-all(bf16[16,160,128]{2,1,0:T(8,128)(2,1)S(1)} %pad_maximum_fusion), channel_id=1, replica_groups=mesh['sp'=16,'tp'=16] {'sp'}, dimensions={0} | all-to-all | bytes 1310720 | tf_op jit(solution)/shard_map/all_to_all | solution.py:32
  38.5 71.1 %all-gather.2.cloned.1.call-done = bf16[2560,2048]{1,0:T(8,128)(2,1)} async-done(((bf16[2560,128]{1,0:T(8,128)(2,1)}), bf16[2560,2048]{1,0:T(8,128)(2,1)}) %all-gather.2.cloned.1.call-update) | async-done | bytes 10485776 | tf_op jit(solution)/shard_map/all_gather | solution.py:22
  109.6 4.2 %fusion.13 = f32[1280,128]{1,0:T(8,128)S(1)} fusion(bf16[2560,2048]{1,0:T(8,128)(2,1)} %all-gather.2.cloned.1.call-done, bf16[1,128,2048]{2,1,0:T(8,128)(2,1)S(1)} %copy-done), kind=kOutput, calls=%fused_computation.24 | convolution fusion | flops 671088640 | bytes 6422528 | tf_op jit(solution)/shard_map/dot_general | solution.py:112
  115.1 1.6 fusion.15
  116.7 1.7 multiply_convert_fusion.1
  118.5 1.5 fusion.37
  120.0 3.8 %fusion.4 = bf16[2048,1280]{0,1:T(8,128)(2,1)} fusion(f32[1280,2048]{1,0:T(8,128)S(1)} %fusion.37, bf16[1280,128]{1,0:T(8,128)(2,1)S(1)} %get-tuple-element.434, bf16[1,128,2048]{2,1,0:T(8,128)(2,1)S(1)} %copy-done.14), kind=kOutput, calls=%fused_computation.15 | convolution fusion | flops 676331520 | bytes 16580608 | tf_op jit(solution)/shard_map/dot_general | solution.py:150
  123.8 7.9 %copy.221 = bf16[2048,1280]{1,0:T(8,128)(2,1)} copy(bf16[2048,1280]{0,1:T(8,128)(2,1)} %fusion.4) | data formatting | bytes 10485760
  135.0 6.0 %all-to-all-start.3 = ((bf16[16,65,128]{2,1,0:T(8,128)(2,1)}), bf16[16,65,128]{2,1,0:T(8,128)(2,1)S(1)}, u32[]{:S(2)}, u32[]{:S(2)}) async-start(bf16[16,65,128]{2,1,0:T(8,128)(2,1)} %broadcast_in_dim.136), calls=%async_computation.3 | async-start | bytes 589824 | tf_op jit(solution)/shard_map/all_to_all | solution.py:38
  142.2 50.3 %reduce-scatter.4.cloned.1.call-done = bf16[128,1280]{1,0:T(8,128)(2,1)} async-done(((bf16[2048,1280]{1,0:T(8,128)(2,1)}), bf16[128,1280]{1,0:T(8,128)(2,1)}) %reduce-scatter.4.cloned.1.call-update) | async-done | bytes 327696
  192.5 1.9 copy.222
  194.4 6.6 %all-to-all-start.1 = ((bf16[128,16,80]{0,2,1:T(8,128)(2,1)}), bf16[128,16,80]{0,2,1:T(8,128)(2,1)S(1)}, u32[]{:S(2)}, u32[]{:S(2)}) async-start(bf16[128,16,80]{0,2,1:T(8,128)(2,1)} %bitcast.12), calls=%async_computation.1 | async-start | bytes 655360 | tf_op jit(solution)/shard_map/all_to_all | solution.py:244
  202.0 8.1 %all-to-all-done.1 = bf16[128,16,80]{0,2,1:T(8,128)(2,1)S(1)} async-done(((bf16[128,16,80]{0,2,1:T(8,128)(2,1)}), bf16[128,16,80]{0,2,1:T(8,128)(2,1)S(1)}, u32[]{:S(2)}, u32[]{:S(2)}) %all-to-all-start.1) | async-done | bytes 327712 | tf_op jit(solution)/shard_map/all_to_all | solution.py:244
  211.8 8.0 %all-to-all-start.2 = ((bf16[16,320,128]{2,1,0:T(8,128)(2,1)}), bf16[16,320,128]{2,1,0:T(8,128)(2,1)S(1)}, u32[]{:S(2)}, u32[]{:S(2)}) async-start(bf16[16,320,128]{2,1,0:T(8,128)(2,1)} %stack.2), calls=%async_computation.2 | async-start | bytes 2621440 | tf_op jit(solution)/shard_map/all_to_all | solution.py:16
  222.7 4.5 %fusion.21 = f32[1,128,2048]{2,1,0:T(8,128)} fusion(bf16[1280,128]{1,0:T(8,128)(2,1)} %copy-done.10, bf16[2560,2048]{1,0:T(8,128)(2,1)} %all-gather.2.cloned.1.call-done), kind=kOutput, calls=%fused_computation.32 | convolution fusion | flops 671088640 | bytes 6619136 | tf_op jit(solution)/shard_map/dot_general | solution.py:106
  227.2 4.3 %fusion.18 = f32[1,128,2048]{2,1,0:T(8,128)} fusion(bf16[1280,128]{1,0:T(8,128)(2,1)S(1)} %get-tuple-element.435, bf16[2560,2048]{1,0:T(8,128)(2,1)} %all-gather.2.cloned.1.call-done), kind=kOutput, calls=%fused_computation.31 | convolution fusion | flops 671088640 | bytes 6619136 | tf_op jit(solution)/shard_map/dot_general | solution.py:106
  231.6 4.4 %fusion.24 = f32[1,128,2048]{2,1,0:T(8,128)} fusion(bf16[2560,2048]{1,0:T(8,128)(2,1)} %all-gather.2.cloned.1.call-done, f32[1280,128]{1,0:T(8,128)S(1)} %copy-done.29, f32[1280,128]{1,0:T(8,128)S(1)} %copy-done.27), kind=kOutput, calls=%fused_computation.33 | convolution fusion | flops 672071680 | bytes 7602176 | tf_op jit(solution)/shard_map/dot_general | solution.py:106
  235.9 14.1 %all-to-all-done.2 = bf16[16,320,128]{2,1,0:T(8,128)(2,1)S(1)} async-done(((bf16[16,320,128]{2,1,0:T(8,128)(2,1)}), bf16[16,320,128]{2,1,0:T(8,128)(2,1)S(1)}, u32[]{:S(2)}, u32[]{:S(2)}) %all-to-all-start.2) | async-done | bytes 1310752 | tf_op jit(solution)/shard_map/all_to_all | solution.py:16
  250.0 1.9 copy.195
  252.0 2.4 reshape.482
  254.3 1.5 fusion.35
  255.9 2.1 fusion.87
  259.4 9.9 %while.42 = (s32[]{:T(128)}, f32[1,64]{1,0:T(1,128)}, f32[1,64,128]{2,1,0:T(8,128)S(1)}, f32[5,1,64]{2,0,1:T(8,128)S(1)}, f32[5,1,64,128]{3,2,1,0:T(8,128)S(1)},...) while((s32[]{:T(128)}, f32[1,64]{1,0:T(1,128)}, ...), condition=%wide.region_12.13_spmd.clone, body=%wide.region_11.12_spmd.clone.sunk | while | flops 32900 | bytes 166297 | solution.py:267
  270.7 3.7 %all-to-all-start.5 = ((bf16[16,65,128]{2,1,0:T(8,128)(2,1)}), bf16[16,65,128]{2,1,0:T(8,128)(2,1)S(1)}, u32[]{:S(2)}, u32[]{:S(2)}) async-start(bf16[16,65,128]{2,1,0:T(8,128)(2,1)} %broadcast_in_dim.141), calls=%async_computation.5 | async-start | bytes 589824 | tf_op jit(solution)/shard_map/all_to_all | solution.py:38
  276.9 7.3 %all-to-all-done.5 = bf16[16,65,128]{2,1,0:T(8,128)(2,1)S(1)} async-done(((bf16[16,65,128]{2,1,0:T(8,128)(2,1)}), bf16[16,65,128]{2,1,0:T(8,128)(2,1)S(1)}, u32[]{:S(2)}, u32[]{:S(2)}) %all-to-all-start.5) | async-done | bytes 266272 | tf_op jit(solution)/shard_map/all_to_all | solution.py:38
  286.7 1.5 fusion.50
  288.1 1.4 fusion.32
  289.9 1.4 convolution_convert_fusion
  291.3 3.6 %all-to-all-start.4 = ((bf16[16,128,128]{2,1,0:T(8,128)(2,1)}), bf16[16,128,128]{2,1,0:T(8,128)(2,1)S(1)}, u32[]{:S(2)}, u32[]{:S(2)}) async-start(bf16[16,128,128]{2,1,0:T(8,128)(2,1)} %bitcast.292), calls=%async_computation.4 | async-start | bytes 1048576 | tf_op jit(solution)/shard_map/all_to_all | solution.py:97
  302.1 4.0 %all-to-all-done.4 = bf16[16,128,128]{2,1,0:T(8,128)(2,1)S(1)} async-done(((bf16[16,128,128]{2,1,0:T(8,128)(2,1)}), bf16[16,128,128]{2,1,0:T(8,128)(2,1)S(1)}, u32[]{:S(2)}, u32[]{:S(2)}) %all-to-all-start.4) | async-done | bytes 524320 | tf_op jit(solution)/shard_map/all_to_all | solution.py:97
  (233 shorter events, 44.9 us)
Async XLA Ops:
  7.2 102.4 %copy-start = (bf16[1,128,2048]{2,1,0:T(8,128)(2,1)S(1)}, bf16[1,128,2048]{2,1,0:T(8,128)(2,1)}, u32[]{:S(2)}) copy-start(bf16[1,128,2048]{2,1,0:T(8,128)(2,1)} %param.22) | copy-start | bytes 1572868
  7.2 102.4 %all-gather.2.cloned.1.call-start = ((), (), s32[]{:S(2)}) async-start(), calls=%async_computation.7 | async-start | bytes 11141120 | tf_op jit(solution)/shard_map/all_gather | solution.py:22
  38.2 75.5 %copy-start.14 = (bf16[1,128,2048]{2,1,0:T(8,128)(2,1)S(1)}, bf16[1,128,2048]{2,1,0:T(8,128)(2,1)}, u32[]{:S(2)}) copy-start(bf16[1,128,2048]{2,1,0:T(8,128)(2,1)} %param.23) | copy-start | bytes 1572868
  38.2 154.3 %reduce-scatter.4.cloned.1.call-start = ((), (), s32[]{:S(2)}) async-start(), calls=%async_computation.8 | async-start | bytes 5570560
  109.6 5.5 %copy-start.1 = (bf16[2560,2048]{1,0:T(8,128)(2,1)S(1)}, bf16[2560,2048]{1,0:T(8,128)(2,1)}, u32[]{:S(2)}) copy-start(bf16[2560,2048]{1,0:T(8,128)(2,1)} %all-gather.2.cloned.1.call-done) | copy-start | bytes 31457284
  115.1 1.6 copy-start.26
  115.1 1.6 copy-start.25
  116.7 1.8 copy-start.28
  131.7 9.3 %copy-start.18 = (bf16[320,64]{0,1:T(8,128)(2,1)S(1)}, bf16[320,64]{0,1:T(8,128)(2,1)}, u32[]{:S(2)}) copy-start(bf16[320,64]{0,1:T(8,128)(2,1)} %param.26) | copy-start | bytes 122884
  131.7 78.4 %copy-start.17 = (bf16[320,128]{1,0:T(8,128)(2,1)S(1)}, bf16[320,128]{1,0:T(8,128)(2,1)}, u32[]{:S(2)}) copy-start(bf16[320,128]{1,0:T(8,128)(2,1)} %param.18) | copy-start | bytes 245764
  134.2 7.0 %copy-start.7 = (f32[5,1,64,128]{3,2,1,0:T(8,128)}, f32[5,1,64,128]{3,2,1,0:T(8,128)S(1)}, u32[]{:S(2)}) copy-start(f32[5,1,64,128]{3,2,1,0:T(8,128)S(1)} %get-tuple-element.195) | copy-start | bytes 491524
  134.2 87.5 %copy-start.22 = (f32[5,1,64]{2,1,0:T(1,128)}, f32[5,1,64]{2,1,0:T(1,128)S(1)}, u32[]{:S(2)}) copy-start(f32[5,1,64]{2,1,0:T(1,128)S(1)} %get-tuple-element.613) | copy-start | bytes 3844
  134.2 87.5 %copy-start.23 = (f32[1,64]{1,0:T(1,128)}, f32[1,64]{1,0:T(1,128)S(1)}, u32[]{:S(2)}) copy-start(f32[1,64]{1,0:T(1,128)S(1)} %get-tuple-element.194) | copy-start | bytes 772
  135.0 59.4 %all-to-all-start.3 = ((bf16[16,65,128]{2,1,0:T(8,128)(2,1)}), bf16[16,65,128]{2,1,0:T(8,128)(2,1)S(1)}, u32[]{:S(2)}, u32[]{:S(2)}) async-start(bf16[16,65,128]{2,1,0:T(8,128)(2,1)} %broadcast_in_dim.136), calls=%async_computation.3 | async-start | bytes 589824 | tf_op jit(solution)/shard_map/all_to_all | solution.py:38
  141.1 70.7 %copy-start.4 = (f32[320,64]{1,0:T(8,128)}, f32[320,64]{1,0:T(8,128)S(1)}, u32[]{:S(2)}) copy-start(f32[320,64]{1,0:T(8,128)S(1)} %copy.196) | copy-start | bytes 245764
  141.2 70.6 %copy-start.2 = (f32[5,64,64]{2,1,0:T(8,128)}, f32[5,64,64]{2,1,0:T(8,128)S(1)}, u32[]{:S(2)}) copy-start(f32[5,64,64]{2,1,0:T(8,128)S(1)} %fusion.47) | copy-start | bytes 245764
  142.2 85.0 %copy-start.6 = (f32[5,64,64]{2,1,0:T(8,128)}, f32[5,64,64]{2,1,0:T(8,128)S(1)}, u32[]{:S(2)}) copy-start(f32[5,64,64]{2,1,0:T(8,128)S(1)} %convolution_select_fusion.1) | copy-start | bytes 245764
  194.4 17.4 %copy-start.11 = (bf16[16,65,128]{2,1,0:T(8,128)(2,1)}, bf16[16,65,128]{2,1,0:T(8,128)(2,1)S(1)}, u32[]{:S(2)}) copy-start(bf16[16,65,128]{2,1,0:T(8,128)(2,1)S(1)} %all-to-all-done.3) | copy-start | bytes 798724
  194.4 15.7 %all-to-all-start.1 = ((bf16[128,16,80]{0,2,1:T(8,128)(2,1)}), bf16[128,16,80]{0,2,1:T(8,128)(2,1)S(1)}, u32[]{:S(2)}, u32[]{:S(2)}) async-start(bf16[128,16,80]{0,2,1:T(8,128)(2,1)} %bitcast.12), calls=%async_computation.1 | async-start | bytes 655360 | tf_op jit(solution)/shard_map/all_to_all | solution.py:244
  211.8 38.2 %all-to-all-start.2 = ((bf16[16,320,128]{2,1,0:T(8,128)(2,1)}), bf16[16,320,128]{2,1,0:T(8,128)(2,1)S(1)}, u32[]{:S(2)}, u32[]{:S(2)}) async-start(bf16[16,320,128]{2,1,0:T(8,128)(2,1)} %stack.2), calls=%async_computation.2 | async-start | bytes 2621440 | tf_op jit(solution)/shard_map/all_to_all | solution.py:16
  222.7 8.9 %copy-start.27 = (f32[1280,128]{1,0:T(8,128)S(1)}, f32[1280,128]{1,0:T(8,128)}, u32[]{:S(2)}) copy-start(f32[1280,128]{1,0:T(8,128)} %copy-done.26) | copy-start | bytes 1966084
  222.7 8.9 %copy-start.29 = (f32[1280,128]{1,0:T(8,128)S(1)}, f32[1280,128]{1,0:T(8,128)}, u32[]{:S(2)}) copy-start(f32[1280,128]{1,0:T(8,128)} %copy-done.28) | copy-start | bytes 1966084
  255.9 2.1 copy-start.3
  270.7 25.5 %copy-start.5 = (f32[320,64]{1,0:T(8,128)S(1)}, f32[320,64]{1,0:T(8,128)}, u32[]{:S(2)}) copy-start(f32[320,64]{1,0:T(8,128)} %copy-done.4) | copy-start | bytes 245764
  270.7 25.5 %copy-start.9 = (bf16[320,128]{1,0:T(8,128)(2,1)S(1)}, bf16[320,128]{1,0:T(8,128)(2,1)}, u32[]{:S(2)}) copy-start(bf16[320,128]{1,0:T(8,128)(2,1)} %param.28) | copy-start | bytes 245764
  270.7 25.5 %copy-start.21 = (f32[5,1,64]{2,0,1:T(8,128)S(1)}, f32[5,1,64]{2,0,1:T(8,128)}, u32[]{:S(2)}) copy-start(f32[5,1,64]{2,0,1:T(8,128)} %copy-done.20) | copy-start | bytes 3844
  270.7 13.6 %all-to-all-start.5 = ((bf16[16,65,128]{2,1,0:T(8,128)(2,1)}), bf16[16,65,128]{2,1,0:T(8,128)(2,1)S(1)}, u32[]{:S(2)}, u32[]{:S(2)}) async-start(bf16[16,65,128]{2,1,0:T(8,128)(2,1)} %broadcast_in_dim.141), calls=%async_computation.5 | async-start | bytes 589824 | tf_op jit(solution)/shard_map/all_to_all | solution.py:38
  289.9 8.5 %copy-start.13 = (f32[2,1,64,128]{3,2,0,1:T(8,128)S(1)}, f32[2,1,64,128]{3,2,0,1:T(8,128)}, u32[]{:S(2)}) copy-start(f32[2,1,64,128]{3,2,0,1:T(8,128)} %multiply_add_fusion.5) | copy-start | bytes 196612
  289.9 8.5 %copy-start.24 = (f32[1,64]{1,0:T(1,128)S(1)}, f32[1,64]{1,0:T(1,128)}, u32[]{:S(2)}) copy-start(f32[1,64]{1,0:T(1,128)} %copy-done.23) | copy-start | bytes 772
  289.9 10.5 %copy-start.16 = (bf16[320,64]{0,1:T(8,128)(2,1)S(1)}, bf16[320,64]{0,1:T(8,128)(2,1)}, u32[]{:S(2)}) copy-start(bf16[320,64]{0,1:T(8,128)(2,1)} %param.29) | copy-start | bytes 122884
  289.9 11.2 %copy-start.12 = (f32[5,64,128]{2,1,0:T(8,128)S(1)}, f32[5,64,128]{2,1,0:T(8,128)}, u32[]{:S(2)}) copy-start(f32[5,64,128]{2,1,0:T(8,128)} %fusion.87) | copy-start | bytes 491524
  291.3 14.8 %all-to-all-start.4 = ((bf16[16,128,128]{2,1,0:T(8,128)(2,1)}), bf16[16,128,128]{2,1,0:T(8,128)(2,1)S(1)}, u32[]{:S(2)}, u32[]{:S(2)}) async-start(bf16[16,128,128]{2,1,0:T(8,128)(2,1)} %bitcast.292), calls=%async_computation.4 | async-start | bytes 1048576 | tf_op jit(solution)/shard_map/all_to_all | solution.py:97
  (5 other events, 5.5 us)
Sparse Core Ops, SparseCore 0:
  38.4 71.1 all-gather.1
  131.8 60.6 reduce-scatter.3
